TPU v7x, 32 devices: a whole 2x2x4 slice. The times are simulated.
32 devices in a mesh: grp: 2 (over y), sp: 4 (over z), tp: 4 (over x, core).
Axes of the slice: x: 2, y: 2, z: 4, core: 2. Of those that a mesh axis runs over, the one named last changes fastest.
Arguments:
- tokens: bfloat16 [2048, 4096], P(('grp', 'sp')), parts along dimension 0, may hold values from -6 to 6
- norm_gain: bfloat16 [2, 4096], replicated, may hold values from 0.099609375 to 1.8984375
- w_query: bfloat16 [2, 4096, 2048], P(None, 'sp', 'tp'), may hold values from -0.09375 to 0.09375
- w_key: bfloat16 [2, 4096, 2048], P(None, 'sp', 'tp'), may hold values from -0.09375 to 0.09375
- w_value: bfloat16 [2, 4096, 2048], P(None, 'sp', 'tp'), may hold values from -0.09375 to 0.09375
- w_out: bfloat16 [2, 2048, 4096], P(None, 'tp', 'sp'), may hold values from -0.125 to 0.125
- offset_bias: float32 [2, 16, 15, 31], P(None, 'tp'), may hold values from -4 to 300
Outputs:
- mixed: bfloat16 [2048, 4096], P(('grp', 'sp')), parts along dimension 0
There are 2 independent parts, one for each index of `grp`. A program takes and returns all parts, laid end to end along the dimension named above; an argument that names none is the same for every part. Nothing has to cross between parts.
All inputs are finite; a program needn't handle non-finite values.
Results may differ from a plain program's by a relative error of at most 0.013.
Values may be sent and summed in bfloat16 or wider, within the bound.
No kernel may reach another device: no remote copies, remote signals or barrier semaphores. Data moves between devices by JAX's collectives and lax.ppermute only.
A program may use at most 128 MiB of HBM per device.

v0:
```python
import jax
import jax.numpy as jnp
from jax import lax
from jax.sharding import PartitionSpec as P

HD = 128
GRID_W = 64
KR = 8
KC = 16
LAYERS = 2
norm_eps = 1e-06


def with_halo(block, sides, width):
    for axis, dim in sides:
        count = lax.axis_size(axis)
        forward = [(i, i + 1) for i in range(count - 1)]
        backward = [(target, source) for source, target in forward]
        low = lax.ppermute(
            lax.slice_in_dim(block, block.shape[dim] - width, None, axis=dim), axis, forward
        )
        high = lax.ppermute(lax.slice_in_dim(block, 0, width, axis=dim), axis, backward)
        block = jnp.concatenate([low, block, high], axis=dim)
    return block


def rms_rows(values, gain):
    wide = values.astype(jnp.float32)
    scaled = wide * lax.rsqrt(jnp.mean(wide * wide, axis=-1, keepdims=True) + norm_eps)
    return (scaled * gain.astype(jnp.float32)).astype(jnp.bfloat16)


def on_device(tokens, norm_gain, w_query, w_key, w_value, w_out, offset_bias):
    sp_count = lax.axis_size("sp")
    sp_index = lax.axis_index("sp")
    tok_rows = tokens.shape[0]
    local_rows = tok_rows // GRID_W
    grid_rows = local_rows * sp_count
    heads_here = offset_bias.shape[1]
    head_width = heads_here * HD
    reach = KR // 2
    scale = HD ** (-0.5)
    columns = jnp.arange(GRID_W, dtype=jnp.int32)
    col_first = jnp.clip(columns - KC // 2, 0, GRID_W - KC)
    col_inside = (columns[None, :] >= col_first[:, None]) & (
        columns[None, :] < col_first[:, None] + KC
    )
    col_offset = jnp.clip(columns[None, :] - columns[:, None], 1 - KC, KC - 1) + KC - 1
    col_onehot = (
        jnp.arange(2 * KC - 1, dtype=jnp.int32)[:, None, None] == col_offset[None, :, :]
    ).astype(jnp.float32)
    first_row = sp_index * local_rows
    own_rows = first_row + jnp.arange(local_rows, dtype=jnp.int32)
    row_first = jnp.clip(own_rows - reach, 0, grid_rows - KR)
    band_start = row_first - first_row + reach
    row_offset = (
        row_first[:, None] + jnp.arange(KR, dtype=jnp.int32)[None, :] - own_rows[:, None] + KR - 1
    )
    row_onehot = (
        row_offset[:, :, None] == jnp.arange(2 * KR - 1, dtype=jnp.int32)[None, None, :]
    ).astype(jnp.float32)
    every_query, every_key, every_value, every_out = (
        lax.all_gather(w_query, "sp", axis=1, tiled=True),
        lax.all_gather(w_key, "sp", axis=1, tiled=True),
        lax.all_gather(w_value, "sp", axis=1, tiled=True),
        lax.all_gather(w_out, "sp", axis=2, tiled=True),
    )
    residual = tokens
    for layer_index in range(LAYERS):
        normed = rms_rows(residual, norm_gain[layer_index])
        queries = jnp.dot(normed, every_query[layer_index], preferred_element_type=jnp.float32)
        keys = jnp.dot(normed, every_key[layer_index], preferred_element_type=jnp.float32)
        values = jnp.dot(normed, every_value[layer_index], preferred_element_type=jnp.float32)
        out_weight = every_out[layer_index]
        queries = queries.astype(jnp.bfloat16).reshape(local_rows, GRID_W, heads_here, HD)
        key_values = jnp.concatenate(
            [keys.astype(jnp.bfloat16), values.astype(jnp.bfloat16)], axis=1
        )
        key_values = key_values.reshape(local_rows, GRID_W, 2 * head_width)
        padded = with_halo(key_values, (("sp", 0),), reach)
        bands = jax.vmap(lambda band_begin: lax.dynamic_slice_in_dim(padded, band_begin, KR, 0))(
            band_start
        )
        band_keys = bands[..., :head_width].reshape(local_rows, KR, GRID_W, heads_here, HD)
        band_values = bands[..., head_width:].reshape(local_rows, KR, GRID_W, heads_here, HD)
        col_bias = jnp.einsum(
            "hro,oqk->hrqk", offset_bias[layer_index], col_onehot, precision=lax.Precision.HIGHEST
        )
        full_bias = jnp.einsum(
            "ijr,hrqk->hiqjk", row_onehot, col_bias, precision=lax.Precision.HIGHEST
        )
        scores = jnp.einsum(
            "iqhd,ijkhd->hiqjk", queries, band_keys, preferred_element_type=jnp.float32
        )
        scores = scores * scale + full_bias
        scores = jnp.where(col_inside[None, None, :, None, :], scores, -jnp.inf)
        flattened = scores.reshape(heads_here, local_rows, GRID_W, KR * GRID_W)
        weights = jax.nn.softmax(flattened, axis=-1).astype(jnp.bfloat16)
        weights = weights.reshape(heads_here, local_rows, GRID_W, KR, GRID_W)
        attended = jnp.einsum(
            "hiqjk,ijkhd->iqhd", weights, band_values, preferred_element_type=jnp.float32
        )
        attended = attended.astype(jnp.bfloat16).reshape(tok_rows, head_width)
        branch = lax.psum(
            jnp.dot(attended, out_weight, preferred_element_type=jnp.float32).astype(jnp.bfloat16),
            "tp",
        ).astype(jnp.float32)
        residual = (residual.astype(jnp.float32) + branch).astype(jnp.bfloat16)
    return residual


def solution(mesh):
    return jax.shard_map(
        on_device,
        mesh=mesh,
        in_specs=(
            P(("grp", "sp"), None),
            P(),
            P(None, "sp", "tp"),
            P(None, "sp", "tp"),
            P(None, "sp", "tp"),
            P(None, "tp", "sp"),
            P(None, "tp", None, None),
        ),
        out_specs=P(("grp", "sp"), None),
        check_vma=False,
    )
```

profile of v0, /device:TPU:0, one launch (start us, length us, event | category | flops | bytes accessed | tf_op | source)
XLA Modules:
  0.0 783.5 jit_solution(1764364375646308337)
XLA Ops:
  10.7 3.8 fusion.30
  14.5 6.0 copy.16
  21.1 140.2 %all-gather.5.cloned.1.call-done = bf16[2,4096,512]{2,1,0:T(8,128)(2,1)} async-done(((bf16[2,1024,512]{2,1,0:T(8,128)(2,1)}), bf16[2,4096,512]{2,1,0:T(8,128)(2,1)}) %all-gather.5.cloned.1.call-update) | async-done | bytes 8388624 | tf_op jit(solution)/shard_map/all_gather | solution.py:64
  161.3 3.5 fusion.54
  164.7 145.9 %all-gather.7.cloned.1.call-done = bf16[2,4096,512]{2,1,0:T(8,128)(2,1)} async-done(((bf16[2,1024,512]{2,1,0:T(8,128)(2,1)}), bf16[2,4096,512]{2,1,0:T(8,128)(2,1)}) %all-gather.7.cloned.1.call-update) | async-done | bytes 8388624 | tf_op jit(solution)/shard_map/all_gather | solution.py:65
  310.7 3.5 fusion.55
  314.2 2.1 collective-permute-start
  316.3 1.5 collective-permute-start.1
  317.8 149.6 %all-gather.9.cloned.1.call-done = bf16[2,4096,512]{2,1,0:T(8,128)(2,1)} async-done(((bf16[2,1024,512]{2,1,0:T(8,128)(2,1)}), bf16[2,4096,512]{2,1,0:T(8,128)(2,1)}) %all-gather.9.cloned.1.call-update) | async-done | bytes 8388624 | tf_op jit(solution)/shard_map/all_gather | solution.py:63
  467.4 3.5 fusion.56
  471.0 2.5 pad_maximum_fusion
  473.5 4.4 gather_fusion
  477.9 3.5 slice_bitcast_fusion.19
  484.9 132.0 %all-gather.11.cloned.1.call-done = bf16[2,512,4096]{2,1,0:T(8,128)(2,1)} async-done(((bf16[2,512,1024]{2,1,0:T(8,128)(2,1)}), bf16[2,512,4096]{2,1,0:T(8,128)(2,1)}) %all-gather.11.cloned.1.call-update) | async-done | bytes 8388624 | tf_op jit(solution)/shard_map/all_gather | solution.py:66
  616.9 4.8 convolution_convert_fusion.1
  621.8 2.4 fusion.71
  624.2 47.2 %all-reduce.4.cloned.1.call-done = bf16[256,4096]{1,0:T(8,128)(2,1)} async-done(((bf16[256,4096]{1,0:T(8,128)(2,1)}), bf16[256,4096]{1,0:T(8,128)(2,1)}) %all-reduce.4.cloned.1.call-update) | async-done | bytes 2097168 | tf_op jit(solution)/shard_map/psum | solution.py:104
  671.5 2.5 fusion.4
  675.0 4.5 fusion.57
  679.5 1.2 fusion.58
  680.8 3.4 collective-permute-start.2
  684.3 1.5 collective-permute-start.3
  685.8 3.9 fusion.28
  689.7 5.8 copy.22
  695.4 4.8 fusion.59
  701.3 2.4 pad_maximum_fusion.1
  703.6 4.2 gather_fusion.1
  707.8 3.1 slice_bitcast_fusion.17
  714.5 1.5 slice-done.1
  715.9 2.6 convolution_convert_fusion
  718.6 53.4 %all-reduce.6.cloned.1.call-done = bf16[256,4096]{1,0:T(8,128)(2,1)} async-done(((bf16[256,4096]{1,0:T(8,128)(2,1)}), bf16[256,4096]{1,0:T(8,128)(2,1)}) %all-reduce.6.cloned.1.call-update) | async-done | bytes 2097168 | tf_op jit(solution)/shard_map/psum | solution.py:104
  771.9 4.7 fusion.7
  (67 shorter events, 13.9 us)
Async XLA Ops:
  6.5 2.9 copy-start.7
  6.5 154.7 %all-gather.5.cloned.1.call-start = ((), (), s32[]{:S(2)}) async-start(), calls=%async_computation | async-start | bytes 10485760 | tf_op jit(solution)/shard_map/all_gather | solution.py:64
  7.3 303.4 %all-gather.7.cloned.1.call-start = ((), (), s32[]{:S(2)}) async-start(), calls=%async_computation.1 | async-start | bytes 10485760 | tf_op jit(solution)/shard_map/all_gather | solution.py:65
  8.0 459.4 %all-gather.9.cloned.1.call-start = ((), (), s32[]{:S(2)}) async-start(), calls=%async_computation.2 | async-start | bytes 10485760 | tf_op jit(solution)/shard_map/all_gather | solution.py:63
  8.7 608.2 %all-gather.11.cloned.1.call-start = ((), (), s32[]{:S(2)}) async-start(), calls=%async_computation.3 | async-start | bytes 10485760 | tf_op jit(solution)/shard_map/all_gather | solution.py:66
  9.3 662.1 %all-reduce.4.cloned.1.call-start = ((), (), s32[]{:S(2)}) async-start(), calls=%async_computation.4 | async-start | bytes 4194304 | tf_op jit(solution)/shard_map/psum | solution.py:104
  14.5 6.0 copy-start
  14.5 6.6 copy-start.6
  314.2 156.7 %collective-permute-start = (bf16[4,64,1024]{2,1,0:T(8,128)(2,1)S(1)}, bf16[4,64,1024]{2,1,0:T(8,128)(2,1)}, u32[]{:S(2)}, u32[]{:S(2)}) collective-permute-start(bf16[4,64,1024]{2,1,0:T(8,128)(2,1)S(1)} %bitcast.150), channel_id=1, source_target_pairs={{0,4},{4,8},{8,12},{1,5},{5,9},{9,13},{2,6},{6,10},{10,14},{3,7},{... | collective-permute-start | bytes 1572872 | tf_op jit(solution)/shard_map/ppermute | solution.py:19
  316.3 154.6 %collective-permute-start.1 = (bf16[4,64,1024]{2,1,0:T(8,128)(2,1)S(1)}, bf16[4,64,1024]{2,1,0:T(8,128)(2,1)}, u32[]{:S(2)}, u32[]{:S(2)}) collective-permute-start(bf16[4,64,1024]{2,1,0:T(8,128)(2,1)S(1)} %bitcast.151), channel_id=1, source_target_pairs={{4,0},{8,4},{12,8},{5,1},{9,5},{13,9},{6,2},{10,6},{14,10},{7,3},{... | collective-permute-start | bytes 1572872 | tf_op jit(solution)/shard_map/ppermute | solution.py:22
  477.9 4.1 copy-start.2
  621.7 150.2 %all-reduce.6.cloned.1.call-start = ((), (), s32[]{:S(2)}) async-start(), calls=%async_computation.5 | async-start | bytes 4194304 | tf_op jit(solution)/shard_map/psum | solution.py:104
  671.5 2.5 copy-start.1
  674.0 5.5 slice-start.2
  674.9 4.5 copy-start.5
  675.0 4.6 slice-start.3
  679.5 6.3 copy-start.4
  680.8 20.4 %collective-permute-start.2 = (bf16[4,64,1024]{2,1,0:T(8,128)(2,1)S(1)}, bf16[4,64,1024]{2,1,0:T(8,128)(2,1)S(1)}, u32[]{:S(2)}, u32[]{:S(2)}) collective-permute-start(bf16[4,64,1024]{2,1,0:T(8,128)(2,1)S(1)} %bitcast.147), channel_id=1, source_target_pairs={{0,4},{4,8},{8,12},{1,5},{5,9},{9,13},{2,6},{6,10},{10,14},{3,7},{... | collective-permute-start | bytes 1572872 | tf_op jit(solution)/shard_map/ppermute | solution.py:19
  684.3 17.0 %collective-permute-start.3 = (bf16[4,64,1024]{2,1,0:T(8,128)(2,1)S(1)}, bf16[4,64,1024]{2,1,0:T(8,128)(2,1)}, u32[]{:S(2)}, u32[]{:S(2)}) collective-permute-start(bf16[4,64,1024]{2,1,0:T(8,128)(2,1)S(1)} %bitcast.148), channel_id=1, source_target_pairs={{4,0},{8,4},{12,8},{5,1},{9,5},{13,9},{6,2},{10,6},{14,10},{7,3},{... | collective-permute-start | bytes 1572872 | tf_op jit(solution)/shard_map/ppermute | solution.py:22
  707.8 3.4 copy-start.3
  712.3 2.2 slice-start
  713.0 2.9 slice-start.1
Sparse Core Ops, SparseCore 0:
  8.9 152.3 all-gather.4
  162.8 147.7 all-gather.6
  312.2 155.1 all-gather.8
  468.8 148.0 all-gather.10
  621.9 49.5 all-reduce.3
  718.7 53.1 all-reduce.5
where the time goes:
time: 784 us; the launch traced here: 783 us
  waiting for transfers between devices  671 us (86%)
  matrix products  43.4 us (6%)
  local copies, waits for them, and re-layouts  31.2 us (4%)
  other arithmetic  15.4 us (2%)
  between operations  13.8 us (2%)
  starting transfers between devices  8.71 us (1%)
    all_gather x1, waiting for transfers between devices, on_device(): lax.all_gather(w_query, 'sp', axis=1, tiled=True)  150 us
    all_gather x1, waiting for transfers between devices, on_device(): lax.all_gather(w_value, 'sp', axis=1, tiled=True)  146 us
    all_gather x1, waiting for transfers between devices, on_device(): lax.all_gather(w_key, 'sp', axis=1, tiled=True)  140 us
    all_gather x1, waiting for transfers between devices, on_device(): lax.all_gather(w_out, 'sp', axis=2, tiled=True)  132 us
    psum x2, waiting for transfers between devices, on_device(): lax.psum(jnp.dot(attended, out_weight, preferred_element_type=jnp.float32...  101 us
  transfers between devices with their start and end apart: 10, of which 6 were waited for; matrix products, arithmetic and copies ran while one was open for 7% of the time, Pallas kernels for 0%

commit v1 on v0

--- a/solution.py
+++ b/solution.py
@@ -9,6 +9,11 @@
 KC = 16
 LAYERS = 2
 norm_eps = 1e-06
+
+
+def gather_and_add(x, mesh_axis):
+    pieces = lax.all_gather(x, mesh_axis)
+    return jnp.sum(pieces, axis=0)
 
 
 def with_halo(block, sides, width):
@@ -101,7 +106,7 @@
             "hiqjk,ijkhd->iqhd", weights, band_values, preferred_element_type=jnp.float32
         )
         attended = attended.astype(jnp.bfloat16).reshape(tok_rows, head_width)
-        branch = lax.psum(
+        branch = gather_and_add(
             jnp.dot(attended, out_weight, preferred_element_type=jnp.float32).astype(jnp.bfloat16),
             "tp",
         ).astype(jnp.float32)

time: 784 us -> 812 us (1.036)
  other arithmetic: 15.4 us -> 29.3 us
  waiting for transfers between devices: 671 us -> 680 us
    all_gather x0 -> x2, waiting for transfers between devices: none -> 111 us  [gather_and_add(): pieces = lax.all_gather(x, mesh_axis)]
    psum x2 -> x0, waiting for transfers between devices: 101 us -> none  [on_device(): lax.psum(jnp.dot(attended, out_weight, preferred_element_type=jnp.float32...]
    reduce_sum x0 -> x2, other arithmetic: none -> 13.8 us  [gather_and_add(): return jnp.sum(pieces, axis=0)]
where the time goes in v1:
time: 812 us; the launch traced here: 811 us
  waiting for transfers between devices  680 us (84%)
  matrix products  43.5 us (5%)
  local copies, waits for them, and re-layouts  31.3 us (4%)
  other arithmetic  29.3 us (4%)
  between operations  13.8 us (2%)
  starting transfers between devices  13.7 us (2%)
    all_gather x1, waiting for transfers between devices, on_device(): lax.all_gather(w_key, 'sp', axis=1, tiled=True)  146 us
    all_gather x1, waiting for transfers between devices, on_device(): lax.all_gather(w_query, 'sp', axis=1, tiled=True)  146 us
    all_gather x1, waiting for transfers between devices, on_device(): lax.all_gather(w_value, 'sp', axis=1, tiled=True)  140 us
    all_gather x1, waiting for transfers between devices, on_device(): lax.all_gather(w_out, 'sp', axis=2, tiled=True)  134 us
    all_gather x2, waiting for transfers between devices, gather_and_add(): pieces = lax.all_gather(x, mesh_axis)  111 us
  transfers between devices with their start and end apart: 10, of which 6 were waited for; matrix products, arithmetic and copies ran while one was open for 7% of the time, Pallas kernels for 0%

profile of v1, /device:TPU:0, one launch (start us, length us, event | category | flops | bytes accessed | tf_op | source)
XLA Modules:
  0.0 811.1 jit_solution(1984601489497481170)
XLA Ops:
  10.7 3.8 fusion.30
  14.5 6.0 copy.16
  21.1 140.2 %all-gather.11.cloned.1.call-done = bf16[2,4096,512]{2,1,0:T(8,128)(2,1)} async-done(((bf16[2,1024,512]{2,1,0:T(8,128)(2,1)}), bf16[2,4096,512]{2,1,0:T(8,128)(2,1)}) %all-gather.11.cloned.1.call-update) | async-done | bytes 8388624 | tf_op jit(solution)/shard_map/all_gather | solution.py:70
  161.3 3.5 fusion.55
  164.7 145.9 %all-gather.9.cloned.1.call-done = bf16[2,4096,512]{2,1,0:T(8,128)(2,1)} async-done(((bf16[2,1024,512]{2,1,0:T(8,128)(2,1)}), bf16[2,4096,512]{2,1,0:T(8,128)(2,1)}) %all-gather.9.cloned.1.call-update) | async-done | bytes 8388624 | tf_op jit(solution)/shard_map/all_gather | solution.py:69
  310.7 3.5 fusion.54
  314.2 1.3 collective-permute-start.1
  315.5 5.4 collective-permute-start
  320.9 145.7 %all-gather.13.cloned.1.call-done = bf16[2,4096,512]{2,1,0:T(8,128)(2,1)} async-done(((bf16[2,1024,512]{2,1,0:T(8,128)(2,1)}), bf16[2,4096,512]{2,1,0:T(8,128)(2,1)}) %all-gather.13.cloned.1.call-update) | async-done | bytes 8388624 | tf_op jit(solution)/shard_map/all_gather | solution.py:68
  466.6 3.5 fusion.56
  470.1 2.5 pad_maximum_fusion
  472.7 4.2 gather_fusion
  476.9 3.7 slice_bitcast_fusion.19
  484.2 134.3 %all-gather.15.cloned.1.call-done = bf16[2,512,4096]{2,1,0:T(8,128)(2,1)} async-done(((bf16[2,512,1024]{2,1,0:T(8,128)(2,1)}), bf16[2,512,4096]{2,1,0:T(8,128)(2,1)}) %all-gather.15.cloned.1.call-update) | async-done | bytes 8388624 | tf_op jit(solution)/shard_map/all_gather | solution.py:71
  618.4 4.8 convolution_convert_fusion.1
  623.5 2.4 fusion.71
  625.9 53.9 %all-gather.17.cloned.1.call-done = bf16[1024,4096]{1,0:T(8,128)(2,1)} async-done(((bf16[256,4096]{1,0:T(8,128)(2,1)}), bf16[1024,4096]{1,0:T(8,128)(2,1)}) %all-gather.17.cloned.1.call-update) | async-done | bytes 8388624 | tf_op jit(solution)/shard_map/all_gather | solution.py:15
  679.8 6.9 reduce_sum.62
  686.7 2.5 fusion.4
  690.2 4.5 fusion.58
  697.4 5.4 collective-permute-start.2
  702.8 3.9 fusion.28
  706.7 5.8 copy.22
  712.4 4.8 fusion.59
  718.2 2.4 pad_maximum_fusion.1
  720.6 4.2 gather_fusion.1
  724.8 3.1 slice_bitcast_fusion.17
  731.5 1.5 slice-done.1
  733.0 2.7 convolution_convert_fusion
  735.7 57.0 %all-gather.19.cloned.1.call-done = bf16[1024,4096]{1,0:T(8,128)(2,1)} async-done(((bf16[256,4096]{1,0:T(8,128)(2,1)}), bf16[1024,4096]{1,0:T(8,128)(2,1)}) %all-gather.19.cloned.1.call-update) | async-done | bytes 8388624 | tf_op jit(solution)/shard_map/all_gather | solution.py:15
  792.6 7.0 reduce_sum.65
  799.6 4.7 fusion.7
  (69 shorter events, 16.8 us)
Async XLA Ops:
  6.5 2.9 copy-start.7
  6.5 154.7 %all-gather.11.cloned.1.call-start = ((), (), s32[]{:S(2)}) async-start(), calls=%async_computation.1 | async-start | bytes 10485760 | tf_op jit(solution)/shard_map/all_gather | solution.py:70
  7.3 303.4 %all-gather.9.cloned.1.call-start = ((), (), s32[]{:S(2)}) async-start(), calls=%async_computation | async-start | bytes 10485760 | tf_op jit(solution)/shard_map/all_gather | solution.py:69
  8.0 458.5 %all-gather.13.cloned.1.call-start = ((), (), s32[]{:S(2)}) async-start(), calls=%async_computation.2 | async-start | bytes 10485760 | tf_op jit(solution)/shard_map/all_gather | solution.py:68
  8.7 609.7 %all-gather.15.cloned.1.call-start = ((), (), s32[]{:S(2)}) async-start(), calls=%async_computation.3 | async-start | bytes 10485760 | tf_op jit(solution)/shard_map/all_gather | solution.py:71
  9.3 670.5 %all-gather.17.cloned.1.call-start = ((), (), s32[]{:S(2)}) async-start(), calls=%async_computation.4 | async-start | bytes 10485760 | tf_op jit(solution)/shard_map/all_gather | solution.py:15
  14.5 6.0 copy-start
  14.5 6.6 copy-start.6
  314.2 155.9 %collective-permute-start.1 = (bf16[4,64,1024]{2,1,0:T(8,128)(2,1)S(1)}, bf16[4,64,1024]{2,1,0:T(8,128)(2,1)}, u32[]{:S(2)}, u32[]{:S(2)}) collective-permute-start(bf16[4,64,1024]{2,1,0:T(8,128)(2,1)S(1)} %bitcast.154), channel_id=1, source_target_pairs={{4,0},{8,4},{12,8},{5,1},{9,5},{13,9},{6,2},{10,6},{14,10},{7,3},{... | collective-permute-start | bytes 1572872 | tf_op jit(solution)/shard_map/ppermute | solution.py:27
  315.5 154.6 %collective-permute-start = (bf16[4,64,1024]{2,1,0:T(8,128)(2,1)S(1)}, bf16[4,64,1024]{2,1,0:T(8,128)(2,1)}, u32[]{:S(2)}, u32[]{:S(2)}) collective-permute-start(bf16[4,64,1024]{2,1,0:T(8,128)(2,1)S(1)} %bitcast.155), channel_id=1, source_target_pairs={{0,4},{4,8},{8,12},{1,5},{5,9},{9,13},{2,6},{6,10},{10,14},{3,7},{... | collective-permute-start | bytes 1572872 | tf_op jit(solution)/shard_map/ppermute | solution.py:24
  476.9 4.3 copy-start.2
  623.2 169.4 %all-gather.19.cloned.1.call-start = ((), (), s32[]{:S(2)}) async-start(), calls=%async_computation.5 | async-start | bytes 10485760 | tf_op jit(solution)/shard_map/all_gather | solution.py:15
  686.7 2.5 copy-start.1
  689.2 5.5 slice-start.2
  690.2 4.5 copy-start.5
  690.2 4.6 slice-start.3
  694.8 8.0 copy-start.4
  696.1 22.1 %collective-permute-start.3 = (bf16[4,64,1024]{2,1,0:T(8,128)(2,1)S(1)}, bf16[4,64,1024]{2,1,0:T(8,128)(2,1)S(1)}, u32[]{:S(2)}, u32[]{:S(2)}) collective-permute-start(bf16[4,64,1024]{2,1,0:T(8,128)(2,1)S(1)} %bitcast.151), channel_id=1, source_target_pairs={{4,0},{8,4},{12,8},{5,1},{9,5},{13,9},{6,2},{10,6},{14,10},{7,3},{... | collective-permute-start | bytes 1572872 | tf_op jit(solution)/shard_map/ppermute | solution.py:27
  697.4 20.8 %collective-permute-start.2 = (bf16[4,64,1024]{2,1,0:T(8,128)(2,1)S(1)}, bf16[4,64,1024]{2,1,0:T(8,128)(2,1)}, u32[]{:S(2)}, u32[]{:S(2)}) collective-permute-start(bf16[4,64,1024]{2,1,0:T(8,128)(2,1)S(1)} %bitcast.152), channel_id=1, source_target_pairs={{0,4},{4,8},{8,12},{1,5},{5,9},{9,13},{2,6},{6,10},{10,14},{3,7},{... | collective-permute-start | bytes 1572872 | tf_op jit(solution)/shard_map/ppermute | solution.py:24
  724.8 3.4 copy-start.3
  729.3 2.2 slice-start
  730.0 2.9 slice-start.1
Sparse Core Ops, SparseCore 0:
  8.9 152.3 all-gather.10
  162.8 147.7 all-gather.8
  312.2 154.2 all-gather.12
  468.0 150.4 all-gather.14
  623.4 56.4 all-gather.16
  735.8 56.8 all-gather.18
